TPU v7x, 32 devices: a whole 2x2x4 slice. The times are simulated.
32 devices in a mesh: ep: 32 (over z, y, x, core).
Axes of the slice: x: 2, y: 2, z: 4, core: 2. Of those that a mesh axis runs over, the one named last changes fastest.
Arguments:
- tokens: bfloat16 [2048, 2048], P('ep'), may hold values from -6 to 6
- conv_state: bfloat16 [2048, 3, 1024], P('ep'), may hold values from -6 to 6
- recur_state: float32 [2048, 1024], P('ep'), may hold values from -6 to 6
- w_branch: bfloat16 [2048, 1024], replicated, may hold values from -0.125 to 0.125
- w_gate: bfloat16 [2048, 1024], replicated, may hold values from -0.125 to 0.125
- conv_taps: float32 [4, 1024], replicated, may hold values from -3 to 3
- rate_blocks: bfloat16 [16, 64, 64], replicated, may hold values from -0.75 to 0.75
- input_blocks: bfloat16 [16, 64, 64], replicated, may hold values from -0.75 to 0.75
- decay_param: float32 [1024], replicated, may hold values from 1.5 to 6.5
- w_mix: bfloat16 [1024, 2048], replicated, may hold values from -0.1875 to 0.1875
- gain_pre: float32 [2048], replicated, may hold values from 0.1 to 1.9
- gain_post: float32 [2048], replicated, may hold values from 0.1 to 1.9
- gain_ffn: float32 [2048], replicated, may hold values from 0.1 to 1.9
- gain_out: float32 [2048], replicated, may hold values from 0.1 to 1.9
- routes: int32 [2048, 2], P('ep'), may hold values from 0 to 31, all different within a row; in each aligned block of 64 rows (0 to 63, 64 to 127, ...) at most 12 rows name the same one
- affinity: float32 [2048, 2], P('ep'), may hold values from 0.05 to 1
- w_expert_gate: bfloat16 [32, 2048, 512], P('ep'), may hold values from -0.125 to 0.125
- w_expert_up: bfloat16 [32, 2048, 512], P('ep'), may hold values from -0.125 to 0.125
- w_expert_down: bfloat16 [32, 512, 2048], P('ep'), may hold values from -0.25 to 0.25
Outputs:
- layer_out: bfloat16 [2048, 2048], P('ep')
- conv_next: bfloat16 [2048, 3, 1024], P('ep')
- state_next: float32 [2048, 1024], P('ep')
Inputs may be any that keep to these rules, and one draw needn't show every extreme that they name: `routes`: each row names 2 different experts. Among the 64 rows of one device no expert is named more than 12 times, and in every draw some device names some expert exactly 12 times.
All inputs are finite; a program needn't handle non-finite values.
Results may differ from a plain program's by a relative error of at most 0.014.
Values may be sent and summed in bfloat16 or wider, within the bound.
A program may use at most 128 MiB of HBM per device.

v0:
```python
import jax
import jax.numpy as jnp
from jax import lax
from jax.sharding import PartitionSpec as P

epsilon = 1e-06
gate_scale = 8.0


def norm_rows(values, gain_vec):
    floats = values.astype(jnp.float32)
    inv_scale = lax.rsqrt(jnp.mean(floats * floats, axis=-1, keepdims=True) + epsilon)
    return floats * inv_scale * gain_vec


def recurrence(
    tokens,
    conv_state,
    recur_state,
    w_branch,
    w_gate,
    conv_taps,
    rate_blocks,
    input_blocks,
    decay_param,
    w_mix,
    gain_pre,
    gain_post,
):
    normed = norm_rows(tokens, gain_pre).astype(jnp.bfloat16)
    branch = jnp.dot(normed, w_branch, preferred_element_type=jnp.float32).astype(jnp.bfloat16)
    gate_act = jnp.dot(normed, w_gate, preferred_element_type=jnp.float32).astype(jnp.bfloat16)
    window = jnp.concatenate([conv_state, branch[:, None, :]], axis=1)
    convolved = jnp.sum(window.astype(jnp.float32) * conv_taps[None], axis=1)
    row_count, branch_width = convolved.shape
    blocks = rate_blocks.shape[0]
    pieces = convolved.reshape(row_count, blocks, branch_width // blocks)
    rate_gate = jax.nn.sigmoid(
        jnp.einsum("snc,ncd->snd", pieces, rate_blocks.astype(jnp.float32)).reshape(
            row_count, branch_width
        )
    )
    inflow = jax.nn.sigmoid(
        jnp.einsum("snc,ncd->snd", pieces, input_blocks.astype(jnp.float32)).reshape(
            row_count, branch_width
        )
    )
    log_decay = -gate_scale * rate_gate * jax.nn.softplus(-decay_param)
    state_next = jnp.exp(log_decay) * recur_state + jnp.sqrt(-jnp.expm1(2.0 * log_decay)) * (
        inflow * convolved
    )
    merged = (state_next * jax.nn.gelu(gate_act.astype(jnp.float32))).astype(jnp.bfloat16)
    mix_out = jnp.dot(merged, w_mix, preferred_element_type=jnp.float32).astype(jnp.bfloat16)
    residual = tokens.astype(jnp.float32) + norm_rows(mix_out, gain_post)
    return (residual, window[:, 1:, :], state_next)


def expert_block(got_rows, got_info, cap_total, w_expert_gate, w_expert_up, w_expert_down):
    slot_count, sources, model_width = got_rows.shape
    counts = got_info[0]
    before = jnp.cumsum(counts) - counts
    allowed = jnp.clip(cap_total - before, 0, counts)
    positions = jnp.arange(slot_count, dtype=jnp.int32)
    keep_mask = positions[:, None] < allowed[None, :]
    row_block = got_rows.reshape(slot_count * sources, model_width)
    gate_part = jnp.dot(row_block, w_expert_gate[0], preferred_element_type=jnp.float32)
    up_part = jnp.dot(row_block, w_expert_up[0], preferred_element_type=jnp.float32)
    hidden = (jax.nn.silu(gate_part) * up_part).astype(jnp.bfloat16)
    outputs = jnp.dot(hidden, w_expert_down[0], preferred_element_type=jnp.float32).astype(
        jnp.bfloat16
    )
    outputs = outputs.reshape(slot_count, sources, model_width)
    return jnp.where(keep_mask[:, :, None], outputs, jnp.zeros_like(outputs))


def shards(
    tokens,
    conv_state,
    recur_state,
    w_branch,
    w_gate,
    conv_taps,
    rate_blocks,
    input_blocks,
    decay_param,
    w_mix,
    gain_pre,
    gain_post,
    gain_ffn,
    gain_out,
    routes,
    affinity,
    w_expert_gate,
    w_expert_up,
    w_expert_down,
):
    residual, conv_next, state_next = recurrence(
        tokens,
        conv_state,
        recur_state,
        w_branch,
        w_gate,
        conv_taps,
        rate_blocks,
        input_blocks,
        decay_param,
        w_mix,
        gain_pre,
        gain_post,
    )
    ffn_in = norm_rows(residual, gain_ffn).astype(jnp.bfloat16)
    seq_count, top_count = routes.shape
    model_width = ffn_in.shape[1]
    experts = lax.axis_size("ep") * w_expert_gate.shape[0]
    capacity = max(2, 3 * seq_count * top_count // lax.axis_size("ep"))
    cap_total = seq_count * top_count // 2
    flat_routes = routes.reshape(-1)
    onehot = (flat_routes[:, None] == jnp.arange(experts, dtype=jnp.int32)[None, :]).astype(
        jnp.int32
    )
    slot_index = jnp.sum(jnp.cumsum(onehot, axis=0) * onehot, axis=1) - 1
    load_counts = jnp.sum(onehot, axis=0)
    slot_target = slot_index * experts + flat_routes
    outgoing = (
        jnp.zeros((capacity * experts, model_width), jnp.bfloat16)
        .at[slot_target]
        .set(jnp.repeat(ffn_in, top_count, axis=0))
    )
    outgoing = outgoing.reshape(capacity, experts, model_width)
    send_info = load_counts[None, :]
    got_rows, got_info = (
        lax.all_to_all(outgoing, "ep", split_axis=1, concat_axis=1, tiled=True),
        lax.all_to_all(send_info, "ep", split_axis=1, concat_axis=1, tiled=True),
    )
    finished = expert_block(
        got_rows, got_info, cap_total, w_expert_gate, w_expert_up, w_expert_down
    )
    gathered = lax.all_to_all(finished, "ep", split_axis=1, concat_axis=1, tiled=True)
    picked = jnp.take(gathered.reshape(capacity * experts, model_width), slot_target, axis=0)
    picked = picked.astype(jnp.float32).reshape(seq_count, top_count, model_width)
    weights = affinity / jnp.sum(affinity, axis=1, keepdims=True)
    combined = jnp.sum(weights[:, :, None] * picked, axis=1)
    layer_out = (residual + norm_rows(combined, gain_out)).astype(jnp.bfloat16)
    return (layer_out, conv_next, state_next)


def solution(mesh):
    return jax.shard_map(
        shards,
        mesh=mesh,
        in_specs=(
            P("ep", None),
            P("ep", None, None),
            P("ep", None),
            P(),
            P(),
            P(),
            P(),
            P(),
            P(),
            P(),
            P(),
            P(),
            P(),
            P(),
            P("ep", None),
            P("ep", None),
            P("ep", None, None),
            P("ep", None, None),
            P("ep", None, None),
        ),
        out_specs=(P("ep", None), P("ep", None, None), P("ep", None)),
        check_vma=False,
    )
```

profile of v0, /device:TPU:0, one launch (start us, length us, event | category | flops | bytes accessed | tf_op | source)
XLA Modules:
  0.0 170.9 jit_solution(7606808229073026035)
XLA Ops:
  0.6 0.0 copy-start
  0.6 0.9 copy.69
  1.6 0.1 eq.15
  1.7 0.1 fusion.54
  1.8 0.2 reduce_window_sum.18
  2.0 0.7 fusion.55
  2.7 0.7 copy.72
  3.4 7.3 %all-to-all-start = ((s32[1,32,1]{2,0,1:T(1,128)}), s32[1,32,1]{2,0,1:T(1,128)S(1)}, u32[]{:S(2)}, u32[]{:S(2)}) async-start(s32[1,32,1]{2,0,1:T(1,128)} %copy.72), calls=%async_computation | async-start | bytes 32768 | tf_op jit(solution)/shard_map/all_to_all | solution.py:133
  10.7 0.7 reshape.196
  11.4 1.1 fusion.31
  12.5 0.0 copy-start.3
  12.5 0.0 copy-start.9
  12.5 0.0 copy-start.22
  12.5 3.2 %fusion.21 = bf16[64,1,1024]{2,0,1:T(8,128)(2,1)S(1)} fusion(bf16[2048,1024]{1,0:T(8,128)(2,1)} %param.22, bf16[64,2048]{1,0:T(8,128)(2,1)} %param.19, f32[2048]{0:T(1024)} %param.29, f32[64]{0:T(128)S(1)} %add_rsqrt_fusion.3), kind=kOutput, calls=%fused_computation.26 | convolution fusion | flops 269025280 | bytes 4595968 | tf_op jit(solution)/shard_map/dot_general | solution.py:31
  15.8 0.1 multiply_reduce_fusion.1
  15.9 0.2 reshape.193
  16.1 0.3 fusion.16
  16.4 0.3 copy.65
  16.7 0.2 div.38
  16.9 1.2 fusion.19
  18.2 0.0 copy-start.1
  18.2 0.3 copy.67
  18.5 0.9 div.40
  19.4 0.7 fusion.56
  20.1 1.3 multiply_add_fusion
  21.3 0.0 copy-start.5
  21.4 0.0 copy-start.7
  21.4 0.0 copy-start.10
  21.4 0.0 copy-start.19
  21.4 5.3 %multiply_reduce_fusion.4 = (f32[64]{0:T(128)S(1)}, f32[64,2048]{1,0:T(8,128)S(1)}) fusion(bf16[1024,2048]{1,0:T(8,128)(2,1)} %param.28, f32[64,1024]{1,0:T(8,128)S(1)} %multiply_add_fusion, bf16[2048,1024]{1,0:T(8,128)(2,1)} %param.23, bf16[64,2048]{1,0:T(8,128)(2,1)S(1)} %copy-done.1, f32[2048]{0:T(1024)} %param.29, f32[64]{0:T(128)} %copy-done.16), kind=kOutput, calls=%fused_computation.50 | convolution fusion | flops 538705856 | bytes 9445888 | tf_op jit(solution)/shard_map/dot_general | solution.py:53
  26.8 0.3 multiply_reduce_fusion.3
  27.1 0.2 multiply_convert_fusion
  27.3 0.0 copy-done.12
  27.3 0.5 fusion.57
  27.8 0.3 broadcast_in_dim.30
  28.1 1.0 reshape.214
  29.1 3.2 %scatter_custom_fusion = bf16[384,2048]{1,0:T(8,128)(2,1)} fusion(s32[128]{0:T(128)} %fusion.57, bf16[128,2048]{1,0:T(8,128)(2,1)} %reshape.214, bf16[]{:T(256)} %constant.60.clone.1), kind=kCustom, calls=%fused_computation.35 | custom fusion | bytes 1573376 | tf_op jit(solution)/shard_map/scatter | solution.py:127
  32.4 3.7 %copy.75 = bf16[12,32,2048]{2,0,1:T(8,128)(2,1)} copy(bf16[12,32,2048]{2,1,0:T(8,128)(2,1)} %bitcast.41) | data formatting | bytes 3145728 | tf_op jit(solution)/shard_map/reshape | solution.py:129
  36.0 6.1 %all-to-all-start.1 = ((bf16[12,32,2048]{2,0,1:T(8,128)(2,1)}), bf16[12,32,2048]{2,0,1:T(8,128)(2,1)}, u32[]{:S(2)}, u32[]{:S(2)}) async-start(bf16[12,32,2048]{2,0,1:T(8,128)(2,1)} %copy.75), calls=%async_computation.1 | async-start | bytes 4194304 | tf_op jit(solution)/shard_map/all_to_all | solution.py:132
  42.2 0.1 reduce-window.8
  42.2 0.1 reduce.1
  42.4 0.7 reduce
  43.0 0.1 iota_compare_fusion.1
  43.1 47.7 %all-to-all-done.1 = bf16[12,32,2048]{2,0,1:T(8,128)(2,1)} async-done(((bf16[12,32,2048]{2,0,1:T(8,128)(2,1)}), bf16[12,32,2048]{2,0,1:T(8,128)(2,1)}, u32[]{:S(2)}, u32[]{:S(2)}) %all-to-all-start.1) | async-done | bytes 1572896 | tf_op jit(solution)/shard_map/all_to_all | solution.py:132
  90.8 2.6 %copy.76 = bf16[12,32,2048]{2,1,0:T(8,128)(2,1)S(1)} copy(bf16[12,32,2048]{2,0,1:T(8,128)(2,1)} %all-to-all-done.1) | data formatting | bytes 3145728 | tf_op jit(solution)/shard_map/all_to_all | solution.py:132
  93.5 1.1 copy-done.2
  94.6 1.9 %fusion.4 = f32[384,512]{1,0:T(8,128)} fusion(bf16[384,2048]{1,0:T(8,128)(2,1)S(1)} %bitcast.42, bf16[1,2048,512]{2,1,0:T(8,128)(2,1)S(1)} %copy-done.21), kind=kOutput, calls=%fused_computation.8 | convolution fusion | flops 805306368 | bytes 4456448 | tf_op jit(solution)/shard_map/dot_general | solution.py:66
  96.5 5.3 %convolution_convert_fusion = bf16[384,2048]{1,0:T(8,128)(2,1)} fusion(bf16[1,512,2048]{2,1,0:T(8,128)(2,1)S(1)} %copy-done, bf16[384,2048]{1,0:T(8,128)(2,1)} %bitcast.43, bf16[1,2048,512]{2,1,0:T(8,128)(2,1)} %param.36, f32[384,512]{1,0:T(8,128)} %fusion.4), kind=kOutput, calls=%fused_computation.2 | convolution fusion | flops 1612578816 | bytes 8126464 | tf_op jit(solution)/shard_map/dot_general | solution.py:69
  101.8 3.7 %copy_select_fusion = bf16[12,32,2048]{2,0,1:T(8,128)(2,1)} fusion(bf16[12,32,2048]{2,1,0:T(8,128)(2,1)} %bitcast.44, pred[12,32]{0,1:T(8,128)(4,1)S(1)} %iota_compare_fusion.1), kind=kLoop, calls=%fused_computation.10 | loop fusion | flops 786432 | bytes 3146112 | tf_op jit(solution)/shard_map/jit(_where)/select_n | solution.py:73
  105.4 0.0 copy-start.4
  105.5 4.1 %all-to-all-start.2 = ((bf16[12,32,2048]{2,0,1:T(8,128)(2,1)}), bf16[12,32,2048]{2,0,1:T(8,128)(2,1)}, u32[]{:S(2)}, u32[]{:S(2)}) async-start(bf16[12,32,2048]{2,0,1:T(8,128)(2,1)} %copy_select_fusion), calls=%async_computation.2 | async-start | bytes 4194304 | tf_op jit(solution)/shard_map/all_to_all | solution.py:138
  109.6 0.1 mul.210
  109.7 0.1 copy.70
  109.8 0.1 copy.71
  110.0 0.7 copy.68
  110.7 0.8 fusion.36
  111.5 46.8 %all-to-all-done.2 = bf16[12,32,2048]{2,0,1:T(8,128)(2,1)} async-done(((bf16[12,32,2048]{2,0,1:T(8,128)(2,1)}), bf16[12,32,2048]{2,0,1:T(8,128)(2,1)}, u32[]{:S(2)}, u32[]{:S(2)}) %all-to-all-start.2) | async-done | bytes 1572896 | tf_op jit(solution)/shard_map/all_to_all | solution.py:138
  158.3 3.6 %copy.78 = bf16[12,32,2048]{2,1,0:T(8,128)(2,1)} copy(bf16[12,32,2048]{2,0,1:T(8,128)(2,1)} %all-to-all-done.2) | data formatting | bytes 3145728 | tf_op jit(solution)/shard_map/all_to_all | solution.py:138
  161.9 3.1 %gather_fusion = bf16[128,2048]{1,0:T(8,128)(2,1)S(1)} fusion(bf16[384,2048]{1,0:T(8,128)(2,1)} %bitcast.40, s32[1024]{0:T(1024)S(1)} %pad_clamp_fusion), kind=kCustom, calls=%fused_computation | custom fusion | bytes 1049088 | tf_op jit(solution)/shard_map/jit(_take)/gather | solution.py:139
  165.0 0.0 copy-start.8
  165.0 1.1 gather.7
  166.1 3.7 %multiply_reduce_fusion = f32[64,2048]{1,0:T(8,128)S(1)} fusion(bf16[64,2,2048]{2,1,0:T(2,128)(2,1)} %gather.7, pred[64,2]{1,0:T(8,128)(4,1)S(1)} %copy.71, f32[64,2]{1,0:T(8,128)S(1)} %copy-done.6), kind=kLoop, calls=%fused_computation.27 | loop fusion | flops 917504 | bytes 1049216 | tf_op jit(solution)/shard_map/reduce_sum | solution.py:142
  169.8 0.1 multiply_reduce_fusion.2
  170.0 0.9 add_convert_fusion
  (44 shorter events, 0.2 us)
Async XLA Ops:
  0.6 95.8 %copy-start = (bf16[1,512,2048]{2,1,0:T(8,128)(2,1)S(1)}, bf16[1,512,2048]{2,1,0:T(8,128)(2,1)}, u32[]{:S(2)}) copy-start(bf16[1,512,2048]{2,1,0:T(8,128)(2,1)} %param.37) | copy-start | bytes 6291460
  3.4 32.6 %all-to-all-start = ((s32[1,32,1]{2,0,1:T(1,128)}), s32[1,32,1]{2,0,1:T(1,128)S(1)}, u32[]{:S(2)}, u32[]{:S(2)}) async-start(s32[1,32,1]{2,0,1:T(1,128)} %copy.72), calls=%async_computation | async-start | bytes 32768 | tf_op jit(solution)/shard_map/all_to_all | solution.py:133
  12.5 3.3 %copy-start.16 = (f32[64]{0:T(128)}, f32[64]{0:T(128)S(1)}, u32[]{:S(2)}) copy-start(f32[64]{0:T(128)S(1)} %add_rsqrt_fusion.3) | copy-start | bytes 772
  12.5 3.3 %copy-start.3 = (bf16[64,3,1024]{2,0,1:T(8,128)(2,1)S(1)}, bf16[64,3,1024]{2,0,1:T(8,128)(2,1)}, u32[]{:S(2)}) copy-start(bf16[64,3,1024]{2,0,1:T(8,128)(2,1)} %param.20) | copy-start | bytes 1179652
  12.5 3.3 %copy-start.9 = (f32[4,1024]{1,0:T(4,128)S(1)}, f32[4,1024]{1,0:T(4,128)}, u32[]{:S(2)}) copy-start(f32[4,1024]{1,0:T(4,128)} %param.24) | copy-start | bytes 49156
  12.5 3.6 %copy-start.22 = (bf16[16,64,64]{2,1,0:T(8,128)(2,1)S(1)}, bf16[16,64,64]{2,1,0:T(8,128)(2,1)}, u32[]{:S(2)}) copy-start(bf16[16,64,64]{2,1,0:T(8,128)(2,1)} %param.25) | copy-start | bytes 393220
  18.2 3.2 %copy-start.1 = (bf16[64,2048]{1,0:T(8,128)(2,1)S(1)}, bf16[64,2048]{1,0:T(8,128)(2,1)}, u32[]{:S(2)}) copy-start(bf16[64,2048]{1,0:T(8,128)(2,1)} %param.19) | copy-start | bytes 786436
  21.3 5.4 %copy-start.5 = (f32[64,1024]{1,0:T(8,128)}, f32[64,1024]{1,0:T(8,128)S(1)}, u32[]{:S(2)}) copy-start(f32[64,1024]{1,0:T(8,128)S(1)} %multiply_add_fusion) | copy-start | bytes 786436
  21.4 5.4 %copy-start.7 = (f32[2048]{0:T(1024)S(1)}, f32[2048]{0:T(1024)}, u32[]{:S(2)}) copy-start(f32[2048]{0:T(1024)} %param.30) | copy-start | bytes 24580
  21.4 5.7 %copy-start.10 = (f32[2048]{0:T(1024)S(1)}, f32[2048]{0:T(1024)}, u32[]{:S(2)}) copy-start(f32[2048]{0:T(1024)} %param.31) | copy-start | bytes 24580
  21.4 5.9 %copy-start.17 = (s32[128]{0:T(128)S(1)}, s32[128]{0:T(128)}, u32[]{:S(2)}) copy-start(s32[128]{0:T(128)} %get-tuple-element.4) | copy-start | bytes 1540
  21.4 5.9 %copy-start.19 = (s32[128,1]{0,1:T(1,128)S(1)}, s32[128,1]{0,1:T(1,128)}, u32[]{:S(2)}) copy-start(s32[128,1]{0,1:T(1,128)} %reshape.196) | copy-start | bytes 1540
  26.8 0.5 copy-start.12
  36.0 54.8 %all-to-all-start.1 = ((bf16[12,32,2048]{2,0,1:T(8,128)(2,1)}), bf16[12,32,2048]{2,0,1:T(8,128)(2,1)}, u32[]{:S(2)}, u32[]{:S(2)}) async-start(bf16[12,32,2048]{2,0,1:T(8,128)(2,1)} %copy.75), calls=%async_computation.1 | async-start | bytes 4194304 | tf_op jit(solution)/shard_map/all_to_all | solution.py:132
  90.8 3.8 %copy-start.21 = (bf16[1,2048,512]{2,1,0:T(8,128)(2,1)S(1)}, bf16[1,2048,512]{2,1,0:T(8,128)(2,1)}, u32[]{:S(2)}) copy-start(bf16[1,2048,512]{2,1,0:T(8,128)(2,1)} %param.35) | copy-start | bytes 6291460
  93.5 1.1 copy-start.2
  105.4 4.1 %copy-start.18 = (s32[128]{0:T(128)S(1)}, s32[128]{0:T(128)}, u32[]{:S(2)}) copy-start(s32[128]{0:T(128)} %get-tuple-element.4) | copy-start | bytes 1540
  105.4 4.4 %copy-start.14 = (s32[64,2]{0,1:T(2,128)S(1)}, s32[64,2]{0,1:T(2,128)}, u32[]{:S(2)}) copy-start(s32[64,2]{0,1:T(2,128)} %param.33) | copy-start | bytes 1540
  105.4 4.5 %copy-start.15 = (f32[64,2]{0,1:T(2,128)S(1)}, f32[64,2]{0,1:T(2,128)}, u32[]{:S(2)}) copy-start(f32[64,2]{0,1:T(2,128)} %param.34) | copy-start | bytes 1540
  105.4 5.3 %copy-start.20 = (s32[128]{0:T(128)S(1)}, s32[128]{0:T(128)}, u32[]{:S(2)}) copy-start(s32[128]{0:T(128)} %fusion.57) | copy-start | bytes 1540
  105.4 5.3 %copy-start.4 = (bf16[64,3,1024]{2,0,1:T(8,128)(2,1)S(1)}, bf16[64,3,1024]{2,0,1:T(8,128)(2,1)}, u32[]{:S(2)}) copy-start(bf16[64,3,1024]{2,0,1:T(8,128)(2,1)} %param.20) | copy-start | bytes 1179652
  105.5 52.8 %all-to-all-start.2 = ((bf16[12,32,2048]{2,0,1:T(8,128)(2,1)}), bf16[12,32,2048]{2,0,1:T(8,128)(2,1)}, u32[]{:S(2)}, u32[]{:S(2)}) async-start(bf16[12,32,2048]{2,0,1:T(8,128)(2,1)} %copy_select_fusion), calls=%async_computation.2 | async-start | bytes 4194304 | tf_op jit(solution)/shard_map/all_to_all | solution.py:138
  161.9 4.2 %copy-start.6 = (f32[64,2]{1,0:T(8,128)S(1)}, f32[64,2]{1,0:T(8,128)}, u32[]{:S(2)}) copy-start(f32[64,2]{1,0:T(8,128)} %copy.68) | copy-start | bytes 1540
  165.0 5.0 %copy-start.8 = (f32[2048]{0:T(1024)S(1)}, f32[2048]{0:T(1024)}, u32[]{:S(2)}) copy-start(f32[2048]{0:T(1024)} %param.30) | copy-start | bytes 24580
  165.0 5.0 %copy-start.11 = (f32[2048]{0:T(1024)S(1)}, f32[2048]{0:T(1024)}, u32[]{:S(2)}) copy-start(f32[2048]{0:T(1024)} %param.32) | copy-start | bytes 24580
  165.0 5.0 %copy-start.13 = (f32[64]{0:T(128)S(1)}, f32[64]{0:T(128)}, u32[]{:S(2)}) copy-start(f32[64]{0:T(128)} %copy-done.12) | copy-start | bytes 772
where the time goes:
time: 172 us; the launch traced here: 171 us
  waiting for transfers between devices  94.5 us (55%)
  local copies, waits for them, and re-layouts  25.2 us (15%)
  starting transfers between devices  17.6 us (10%)
  matrix products  17.3 us (10%)
  other arithmetic  15.3 us (9%)
    all_to_all x1, waiting for transfers between devices, shards(): lax.all_to_all(outgoing, 'ep', split_axis=1, concat_axis=1, tiled=True)  47.7 us
    all_to_all x1, waiting for transfers between devices, shards(): lax.all_to_all(finished, 'ep', split_axis=1, concat_axis=1, tiled=True)  46.8 us
    all_to_all x1, starting transfers between devices, shards(): lax.all_to_all(send_info, 'ep', split_axis=1, concat_axis=1, tiled=True)  7.33 us
    all_to_all x1, starting transfers between devices, shards(): lax.all_to_all(outgoing, 'ep', split_axis=1, concat_axis=1, tiled=True)  6.14 us
    dot_general x1, matrix products, recurrence(): jnp.dot(merged, w_mix, preferred_element_type=jnp.float32)  5.34 us
    dot_general x1, matrix products, expert_block(): jnp.dot(hidden, w_expert_down[0], preferred_element_type=jnp.float32)  5.3 us
    gather x2, local copies, waits for them, and re-layouts, shards(): jnp.take(gathered.reshape(capacity * experts, model_width), slot_target,...  4.19 us
    all_to_all x1, starting transfers between devices, shards(): lax.all_to_all(finished, 'ep', split_axis=1, concat_axis=1, tiled=True)  4.11 us
  transfers between devices with their start and end apart: 3, of which 2 were waited for; matrix products, arithmetic and copies ran while one was open for 16% of the time, Pallas kernels for 0%

commit v1 on v0

--- a/solution.py
+++ b/solution.py
@@ -135,7 +135,9 @@
     finished = expert_block(
         got_rows, got_info, cap_total, w_expert_gate, w_expert_up, w_expert_down
     )
-    gathered = lax.all_to_all(finished, "ep", split_axis=1, concat_axis=1, tiled=True)
+    gathered = jnp.concatenate(
+        lax.all_to_all(jnp.stack(jnp.split(finished, lax.psum(1, "ep"), 1), axis=0), "ep", 0, 0), 1
+    )
     picked = jnp.take(gathered.reshape(capacity * experts, model_width), slot_target, axis=0)
     picked = picked.astype(jnp.float32).reshape(seq_count, top_count, model_width)
     weights = affinity / jnp.sum(affinity, axis=1, keepdims=True)

time: 172 us -> 190 us (1.10)
  local copies, waits for them, and re-layouts: 25.2 us -> 45.1 us
    unnamed x47 -> x78, local copies, waits for them, and re-layouts: 2.19 us -> 21.5 us
    all_to_all x1 -> x0, local copies, waits for them, and re-layouts: 3.61 us -> none  [shards(): lax.all_to_all(finished, 'ep', split_axis=1, concat_axis=1, tiled=True)]
    reshape x0 -> x1, local copies, waits for them, and re-layouts: none -> 3.61 us  [shards(): jnp.concatenate(lax.all_to_all(jnp.stack(jnp.split(finished, lax.psum(1,...]
  transfers between devices with their start and end apart: 3 -> 3, of which waited for: 2 -> 2; matrix products, arithmetic and copies ran while one was open for 16% -> 15% of each run, Pallas kernels for 0% -> 0%
where the time goes in v1:
time: 190 us
  waiting for transfers between devices  94.5 us (50%)
  local copies, waits for them, and re-layouts  45.1 us (24%)
  starting transfers between devices  17.6 us (9%)
  matrix products  17.3 us (9%)
  other arithmetic  14 us (7%)
    all_to_all x1, waiting for transfers between devices, shards(): lax.all_to_all(outgoing, 'ep', split_axis=1, concat_axis=1, tiled=True)  47.7 us
    all_to_all x1, waiting for transfers between devices, shards(): lax.all_to_all(jnp.stack(jnp.split(finished, lax.psum(1, 'ep'), 1), axis=...  46.8 us
    unnamed x78, local copies, waits for them, and re-layouts  21.5 us
    all_to_all x1, starting transfers between devices, shards(): lax.all_to_all(send_info, 'ep', split_axis=1, concat_axis=1, tiled=True)  7.33 us
    all_to_all x1, starting transfers between devices, shards(): lax.all_to_all(outgoing, 'ep', split_axis=1, concat_axis=1, tiled=True)  6.14 us
    dot_general x1, matrix products, recurrence(): jnp.dot(merged, w_mix, preferred_element_type=jnp.float32)  5.34 us
    dot_general x1, matrix products, expert_block(): jnp.dot(hidden, w_expert_down[0], preferred_element_type=jnp.float32)  5.3 us
    gather x2, local copies, waits for them, and re-layouts, shards(): jnp.take(gathered.reshape(capacity * experts, model_width), slot_target,...  4.19 us
  transfers between devices with their start and end apart: 3, of which 2 were waited for; matrix products, arithmetic and copies ran while one was open for 15% of the time, Pallas kernels for 0%

profile of v1, /device:TPU:0, one launch (start us, length us, event | category | flops | bytes accessed | tf_op | source)
XLA Modules:
  0.0 189.5 jit_solution(6916450896216639652)
XLA Ops:
  0.6 0.9 copy.103
  2.0 0.7 fusion.87
  2.7 0.7 copy.106
  3.4 7.3 %all-to-all-start = ((s32[1,32,1]{2,0,1:T(1,128)}), s32[1,32,1]{2,0,1:T(1,128)S(1)}, u32[]{:S(2)}, u32[]{:S(2)}) async-start(s32[1,32,1]{2,0,1:T(1,128)} %copy.106), calls=%async_computation | async-start | bytes 32768 | tf_op jit(solution)/shard_map/all_to_all | solution.py:133
  10.7 0.7 reshape.196
  11.4 1.1 fusion.31
  12.5 3.2 %fusion.21 = bf16[64,1,1024]{2,0,1:T(8,128)(2,1)S(1)} fusion(bf16[2048,1024]{1,0:T(8,128)(2,1)} %param.22, bf16[64,2048]{1,0:T(8,128)(2,1)} %param.19, f32[2048]{0:T(1024)} %param.29, f32[64]{0:T(128)S(1)} %add_rsqrt_fusion.3), kind=kOutput, calls=%fused_computation.26 | convolution fusion | flops 269025280 | bytes 4595968 | tf_op jit(solution)/shard_map/dot_general | solution.py:31
  16.9 1.2 fusion.19
  18.5 0.9 div.40
  19.4 0.7 fusion.88
  20.1 1.3 multiply_add_fusion
  21.4 5.3 %multiply_reduce_fusion.4 = (f32[64]{0:T(128)S(1)}, f32[64,2048]{1,0:T(8,128)S(1)}) fusion(bf16[1024,2048]{1,0:T(8,128)(2,1)} %param.28, f32[64,1024]{1,0:T(8,128)S(1)} %multiply_add_fusion, bf16[2048,1024]{1,0:T(8,128)(2,1)} %param.23, bf16[64,2048]{1,0:T(8,128)(2,1)S(1)} %copy-done.1, f32[2048]{0:T(1024)} %param.29, f32[64]{0:T(128)} %copy-done.16), kind=kOutput, calls=%fused_computation.50 | convolution fusion | flops 538705856 | bytes 9445888 | tf_op jit(solution)/shard_map/dot_general | solution.py:53
  28.1 1.0 reshape.214
  29.1 3.2 %scatter_custom_fusion = bf16[384,2048]{1,0:T(8,128)(2,1)} fusion(s32[128]{0:T(128)} %fusion.89, bf16[128,2048]{1,0:T(8,128)(2,1)} %reshape.214, bf16[]{:T(256)} %constant.60.clone.1), kind=kCustom, calls=%fused_computation.35 | custom fusion | bytes 1573376 | tf_op jit(solution)/shard_map/scatter | solution.py:127
  32.4 3.7 %copy.109 = bf16[12,32,2048]{2,0,1:T(8,128)(2,1)} copy(bf16[12,32,2048]{2,1,0:T(8,128)(2,1)} %bitcast.170) | data formatting | bytes 3145728 | tf_op jit(solution)/shard_map/reshape | solution.py:129
  36.0 6.1 %all-to-all-start.1 = ((bf16[12,32,2048]{2,0,1:T(8,128)(2,1)}), bf16[12,32,2048]{2,0,1:T(8,128)(2,1)}, u32[]{:S(2)}, u32[]{:S(2)}) async-start(bf16[12,32,2048]{2,0,1:T(8,128)(2,1)} %copy.109), calls=%async_computation.1 | async-start | bytes 4194304 | tf_op jit(solution)/shard_map/all_to_all | solution.py:132
  42.4 0.7 reduce
  43.1 47.7 %all-to-all-done.1 = bf16[12,32,2048]{2,0,1:T(8,128)(2,1)} async-done(((bf16[12,32,2048]{2,0,1:T(8,128)(2,1)}), bf16[12,32,2048]{2,0,1:T(8,128)(2,1)}, u32[]{:S(2)}, u32[]{:S(2)}) %all-to-all-start.1) | async-done | bytes 1572896 | tf_op jit(solution)/shard_map/all_to_all | solution.py:132
  90.8 2.6 %copy.110 = bf16[12,32,2048]{2,1,0:T(8,128)(2,1)S(1)} copy(bf16[12,32,2048]{2,0,1:T(8,128)(2,1)} %all-to-all-done.1) | data formatting | bytes 3145728 | tf_op jit(solution)/shard_map/all_to_all | solution.py:132
  93.5 1.1 copy-done.2
  94.6 1.9 fusion.4
  96.5 5.3 %convolution_convert_fusion = bf16[384,2048]{1,0:T(8,128)(2,1)} fusion(bf16[1,512,2048]{2,1,0:T(8,128)(2,1)S(1)} %copy-done, bf16[384,2048]{1,0:T(8,128)(2,1)} %bitcast.172, bf16[1,2048,512]{2,1,0:T(8,128)(2,1)} %param.36, f32[384,512]{1,0:T(8,128)} %fusion.4), kind=kOutput, calls=%fused_computation.2 | convolution fusion | flops 1612578816 | bytes 8126464 | tf_op jit(solution)/shard_map/dot_general | solution.py:69
  101.8 2.4 %copy_select_fusion = bf16[12,32,2048]{2,0,1:T(8,128)(2,1)S(1)} fusion(bf16[12,32,2048]{2,1,0:T(8,128)(2,1)} %bitcast.173, pred[12,32]{0,1:T(8,128)(4,1)S(1)} %iota_compare_fusion.1), kind=kLoop, calls=%fused_computation.10 | loop fusion | flops 786432 | bytes 3146112 | tf_op jit(solution)/shard_map/jit(_where)/select_n | solution.py:73
  104.2 0.6 fusion.85
  104.8 0.6 fusion.84
  105.4 0.6 fusion.83
  106.0 0.6 fusion.82
  106.6 0.6 fusion.81
  107.3 0.6 fusion.80
  107.9 0.6 fusion.79
  108.5 0.6 fusion.78
  109.1 0.6 fusion.77
  109.7 0.6 fusion.76
  110.4 0.6 fusion.75
  111.0 0.6 fusion.74
  111.6 0.6 fusion.73
  112.2 0.6 fusion.72
  112.9 0.6 fusion.71
  113.5 0.6 fusion.70
  114.1 0.6 fusion.69
  114.7 0.6 fusion.68
  115.4 0.6 fusion.67
  116.0 0.6 fusion.66
  116.6 0.6 fusion.65
  117.2 0.6 fusion.64
  117.8 0.6 fusion.63
  118.5 0.6 fusion.62
  119.1 0.6 fusion.61
  119.7 0.6 fusion.60
  120.3 0.6 fusion.59
  121.0 0.6 fusion.58
  121.6 0.6 fusion.57
  122.2 0.6 fusion.56
  122.8 0.6 fusion.55
  123.4 0.6 fusion.54
  124.1 4.1 %all-to-all-start.2 = ((bf16[32,12,1,2048]{3,1,2,0:T(8,128)(2,1)}), bf16[32,12,1,2048]{3,1,2,0:T(8,128)(2,1)}, u32[]{:S(2)}, u32[]{:S(2)}) async-start(bf16[32,12,1,2048]{3,1,2,0:T(8,128)(2,1)} %fusion.54), calls=%async_computation.2 | async-start | bytes 4194304 | tf_op jit(solution)/shard_map/all_to_all | solution.py:139
  128.6 0.7 copy.102
  129.3 0.8 fusion.36
  130.1 46.8 %all-to-all-done.2 = bf16[32,12,1,2048]{3,1,2,0:T(8,128)(2,1)} async-done(((bf16[32,12,1,2048]{3,1,2,0:T(8,128)(2,1)}), bf16[32,12,1,2048]{3,1,2,0:T(8,128)(2,1)}, u32[]{:S(2)}, u32[]{:S(2)}) %all-to-all-start.2) | async-done | bytes 1572896 | tf_op jit(solution)/shard_map/all_to_all | solution.py:139
  176.9 3.6 %copy.112 = bf16[12,32,1,2048]{3,1,0,2:T(8,128)(2,1)} copy(bf16[12,32,1,2048]{3,0,2,1:T(8,128)(2,1)} %bitcast.45) | data formatting | bytes 3145728 | tf_op jit(solution)/shard_map/reshape | solution.py:138
  180.5 3.1 %gather_fusion = bf16[128,2048]{1,0:T(8,128)(2,1)S(1)} fusion(bf16[384,2048]{1,0:T(8,128)(2,1)} %bitcast.169, s32[1024]{0:T(1024)S(1)} %pad_clamp_fusion), kind=kCustom, calls=%fused_computation | custom fusion | bytes 1049088 | tf_op jit(solution)/shard_map/jit(_take)/gather | solution.py:141
  183.6 1.1 gather.7
  184.7 3.7 %multiply_reduce_fusion = f32[64,2048]{1,0:T(8,128)S(1)} fusion(bf16[64,2,2048]{2,1,0:T(2,128)(2,1)} %gather.7, pred[64,2]{1,0:T(8,128)(4,1)S(1)} %copy.105, f32[64,2]{1,0:T(8,128)S(1)} %copy-done.6), kind=kLoop, calls=%fused_computation.27 | loop fusion | flops 917504 | bytes 1049216 | tf_op jit(solution)/shard_map/reduce_sum | solution.py:144
  188.6 0.9 add_convert_fusion
  (76 shorter events, 4.0 us)
Async XLA Ops:
  0.6 95.8 %copy-start = (bf16[1,512,2048]{2,1,0:T(8,128)(2,1)S(1)}, bf16[1,512,2048]{2,1,0:T(8,128)(2,1)}, u32[]{:S(2)}) copy-start(bf16[1,512,2048]{2,1,0:T(8,128)(2,1)} %param.37) | copy-start | bytes 6291460
  3.4 32.6 %all-to-all-start = ((s32[1,32,1]{2,0,1:T(1,128)}), s32[1,32,1]{2,0,1:T(1,128)S(1)}, u32[]{:S(2)}, u32[]{:S(2)}) async-start(s32[1,32,1]{2,0,1:T(1,128)} %copy.106), calls=%async_computation | async-start | bytes 32768 | tf_op jit(solution)/shard_map/all_to_all | solution.py:133
  12.5 3.3 %copy-start.16 = (f32[64]{0:T(128)}, f32[64]{0:T(128)S(1)}, u32[]{:S(2)}) copy-start(f32[64]{0:T(128)S(1)} %add_rsqrt_fusion.3) | copy-start | bytes 772
  12.5 3.3 %copy-start.3 = (bf16[64,3,1024]{2,0,1:T(8,128)(2,1)S(1)}, bf16[64,3,1024]{2,0,1:T(8,128)(2,1)}, u32[]{:S(2)}) copy-start(bf16[64,3,1024]{2,0,1:T(8,128)(2,1)} %param.20) | copy-start | bytes 1179652
  12.5 3.3 %copy-start.9 = (f32[4,1024]{1,0:T(4,128)S(1)}, f32[4,1024]{1,0:T(4,128)}, u32[]{:S(2)}) copy-start(f32[4,1024]{1,0:T(4,128)} %param.24) | copy-start | bytes 49156
  12.5 3.6 %copy-start.22 = (bf16[16,64,64]{2,1,0:T(8,128)(2,1)S(1)}, bf16[16,64,64]{2,1,0:T(8,128)(2,1)}, u32[]{:S(2)}) copy-start(bf16[16,64,64]{2,1,0:T(8,128)(2,1)} %param.25) | copy-start | bytes 393220
  18.2 3.2 %copy-start.1 = (bf16[64,2048]{1,0:T(8,128)(2,1)S(1)}, bf16[64,2048]{1,0:T(8,128)(2,1)}, u32[]{:S(2)}) copy-start(bf16[64,2048]{1,0:T(8,128)(2,1)} %param.19) | copy-start | bytes 786436
  21.3 5.4 %copy-start.5 = (f32[64,1024]{1,0:T(8,128)}, f32[64,1024]{1,0:T(8,128)S(1)}, u32[]{:S(2)}) copy-start(f32[64,1024]{1,0:T(8,128)S(1)} %multiply_add_fusion) | copy-start | bytes 786436
  21.4 5.4 %copy-start.7 = (f32[2048]{0:T(1024)S(1)}, f32[2048]{0:T(1024)}, u32[]{:S(2)}) copy-start(f32[2048]{0:T(1024)} %param.30) | copy-start | bytes 24580
  21.4 5.7 %copy-start.10 = (f32[2048]{0:T(1024)S(1)}, f32[2048]{0:T(1024)}, u32[]{:S(2)}) copy-start(f32[2048]{0:T(1024)} %param.31) | copy-start | bytes 24580
  21.4 5.9 %copy-start.17 = (s32[128]{0:T(128)S(1)}, s32[128]{0:T(128)}, u32[]{:S(2)}) copy-start(s32[128]{0:T(128)} %get-tuple-element.4) | copy-start | bytes 1540
  21.4 5.9 %copy-start.19 = (s32[128,1]{0,1:T(1,128)S(1)}, s32[128,1]{0,1:T(1,128)}, u32[]{:S(2)}) copy-start(s32[128,1]{0,1:T(1,128)} %reshape.196) | copy-start | bytes 1540
  26.8 0.5 copy-start.12
  36.0 54.8 %all-to-all-start.1 = ((bf16[12,32,2048]{2,0,1:T(8,128)(2,1)}), bf16[12,32,2048]{2,0,1:T(8,128)(2,1)}, u32[]{:S(2)}, u32[]{:S(2)}) async-start(bf16[12,32,2048]{2,0,1:T(8,128)(2,1)} %copy.109), calls=%async_computation.1 | async-start | bytes 4194304 | tf_op jit(solution)/shard_map/all_to_all | solution.py:132
  90.8 3.8 %copy-start.21 = (bf16[1,2048,512]{2,1,0:T(8,128)(2,1)S(1)}, bf16[1,2048,512]{2,1,0:T(8,128)(2,1)}, u32[]{:S(2)}) copy-start(bf16[1,2048,512]{2,1,0:T(8,128)(2,1)} %param.35) | copy-start | bytes 6291460
  93.5 1.2 copy-start.2
  124.1 4.1 %copy-start.18 = (s32[128]{0:T(128)S(1)}, s32[128]{0:T(128)}, u32[]{:S(2)}) copy-start(s32[128]{0:T(128)} %get-tuple-element.4) | copy-start | bytes 1540
  124.1 4.3 %copy-start.14 = (s32[64,2]{0,1:T(2,128)S(1)}, s32[64,2]{0,1:T(2,128)}, u32[]{:S(2)}) copy-start(s32[64,2]{0,1:T(2,128)} %param.33) | copy-start | bytes 1540
  124.1 4.5 %copy-start.15 = (f32[64,2]{0,1:T(2,128)S(1)}, f32[64,2]{0,1:T(2,128)}, u32[]{:S(2)}) copy-start(f32[64,2]{0,1:T(2,128)} %param.34) | copy-start | bytes 1540
  124.1 5.2 %copy-start.20 = (s32[128]{0:T(128)S(1)}, s32[128]{0:T(128)}, u32[]{:S(2)}) copy-start(s32[128]{0:T(128)} %fusion.89) | copy-start | bytes 1540
  124.1 5.3 %copy-start.4 = (bf16[64,3,1024]{2,0,1:T(8,128)(2,1)S(1)}, bf16[64,3,1024]{2,0,1:T(8,128)(2,1)}, u32[]{:S(2)}) copy-start(bf16[64,3,1024]{2,0,1:T(8,128)(2,1)} %param.20) | copy-start | bytes 1179652
  124.1 52.8 %all-to-all-start.2 = ((bf16[32,12,1,2048]{3,1,2,0:T(8,128)(2,1)}), bf16[32,12,1,2048]{3,1,2,0:T(8,128)(2,1)}, u32[]{:S(2)}, u32[]{:S(2)}) async-start(bf16[32,12,1,2048]{3,1,2,0:T(8,128)(2,1)} %fusion.54), calls=%async_computation.2 | async-start | bytes 4194304 | tf_op jit(solution)/shard_map/all_to_all | solution.py:139
  180.5 4.2 %copy-start.6 = (f32[64,2]{1,0:T(8,128)S(1)}, f32[64,2]{1,0:T(8,128)}, u32[]{:S(2)}) copy-start(f32[64,2]{1,0:T(8,128)} %copy.102) | copy-start | bytes 1540
  183.6 5.0 %copy-start.8 = (f32[2048]{0:T(1024)S(1)}, f32[2048]{0:T(1024)}, u32[]{:S(2)}) copy-start(f32[2048]{0:T(1024)} %param.30) | copy-start | bytes 24580
  183.6 5.0 %copy-start.11 = (f32[2048]{0:T(1024)S(1)}, f32[2048]{0:T(1024)}, u32[]{:S(2)}) copy-start(f32[2048]{0:T(1024)} %param.32) | copy-start | bytes 24580
  183.6 5.0 %copy-start.13 = (f32[64]{0:T(128)S(1)}, f32[64]{0:T(128)}, u32[]{:S(2)}) copy-start(f32[64]{0:T(128)} %copy-done.12) | copy-start | bytes 772
